TPU v7x, 512 devices: a whole 4x4x16 slice. The times are simulated.
512 devices in a mesh: vp: 128 (over z, x, core), dp: 4 (over y).
Axes of the slice: x: 4, y: 4, z: 16, core: 2. Of those that a mesh axis runs over, the one named last changes fastest.
Arguments:
- stream: bfloat16 [1024, 2048], P(('dp', 'vp')), may hold values from -60 to 60
- hidden: bfloat16 [1024, 5632], P('dp', 'vp'), may hold values from -6 to 6
- w_down: bfloat16 [5632, 2048], P(None, 'vp'), may hold values from -0.078125 to 0.078125
- final_gain: float32 [2048], replicated, may hold values from 0.1 to 1.9
- vocab: bfloat16 [2048, 32768], P(None, 'vp'), may hold values from -2 to 200
- vocab_bias: float32 [32768], P('vp'), may hold values from -5 to 5
- targets: int32 [1024], P('dp'), may hold values from 0 to 32767
Outputs:
- losses: float32 [1024], P(('dp', 'vp'))
- grad_input: float32 [1024, 2048], P(('dp', 'vp'))
- grad_vocab: float32 [2048, 32768], P('dp', 'vp')
All inputs are finite; a program needn't handle non-finite values.
Results may differ from a plain program's by a relative error of at most 0.02.
Values may be sent and summed in bfloat16 or wider, within the bound.
No kernel may reach another device: no remote copies, remote signals or barrier semaphores. Data moves between devices by JAX's collectives and lax.ppermute only.
A program may use at most 64 MiB of HBM per device.

v0:
```python
import jax
import jax.numpy as jnp
from jax import lax
from jax.sharding import Mesh
from jax.sharding import PartitionSpec as P

VP = ("vp_0", "vp_1", "vp_2")
DP_VP = ("dp", "vp_0", "vp_1", "vp_2")


norm_eps = 1e-06
zloss_weight = 0.001


def joined_along(pieces, dim):
    pieces = jnp.moveaxis(pieces, 0, dim)
    lengths = pieces.shape
    return pieces.reshape(*lengths[:dim], lengths[dim] * lengths[dim + 1], *lengths[dim + 2 :])


def gather_in_order(array, axes, turns):
    pieces = array[None]
    for k in turns:
        pieces = lax.all_gather(pieces, axes[k], axis=0, tiled=True)
    held = [lax.axis_size(axes[k]) for k in reversed(turns)]
    pieces = pieces.reshape(*held, *array.shape)
    turned = sorted(range(len(turns)), key=lambda place: turns[len(turns) - 1 - place])
    return pieces.transpose(*turned, *range(len(turns), pieces.ndim)).reshape(-1, *array.shape)


def whole_of(array, axes, turns, dim):
    return joined_along(gather_in_order(array, axes, turns), dim)


def collected_together(array, axis):
    leaves = jax.tree.leaves(array)
    turns = sorted(range(len(leaves)), key=lambda k: -leaves[k].size)
    width = (1, *leaves[turns[0]].shape)[-1]
    lines = [
        jnp.pad(leaves[k].reshape(-1), (0, -leaves[k].size % width)).reshape(-1, width)
        for k in turns
    ]
    both, at, found = (lax.all_gather(jnp.concatenate(lines), axis), 0, {})
    for k, line in zip(turns, lines):
        section = both[:, at : at + len(line)].reshape(len(both), -1)
        found[k] = section[:, : leaves[k].size].reshape(-1, *leaves[k].shape)
        at += len(line)
    numbers = iter(range(len(leaves)))
    return jax.tree.map(lambda _: found[next(numbers)], array)


def merged_by_axis(array, axes, combine):
    for axis in axes:
        pieces = collected_together(array, axis)
        array = jax.tree.map(lambda part: part[0], pieces)
        for k in range(1, lax.axis_size(axis)):
            array = combine(array, jax.tree.map(lambda part: part[k], pieces))
    return array


def sent_together(arrays, axis, dim, along):
    ends, at = ([], 0)
    for a in arrays[:-1]:
        at += a.shape[along]
        ends.append(at)
    both = jnp.concatenate(arrays, axis=along)
    return tuple(jnp.split(lax.all_gather(both, axis, axis=dim, tiled=True), ends, axis=along))


def combine_stats(first, second):
    top = jnp.maximum(first[0], second[0])
    total = first[1] * jnp.exp(first[0] - top) + second[1] * jnp.exp(second[0] - top)
    return (top, total, first[2] + second[2])


def body(stream, hidden, w_down, final_gain, vocab, vocab_bias, targets):
    rows_dev = stream.shape[0]
    width = stream.shape[1]
    group = targets.shape[0]
    mine = lax.axis_index(VP)
    w_rows = lax.all_to_all(w_down, VP, split_axis=0, concat_axis=1, tiled=True)
    partial_value = jnp.dot(hidden, w_rows, preferred_element_type=jnp.float32)
    arrived = lax.all_to_all(partial_value[:, None, :], VP, split_axis=0, concat_axis=1, tiled=True)
    proj = jnp.sum(arrived, axis=1)
    normin = (stream.astype(jnp.float32) + proj).astype(jnp.bfloat16)
    values = normin.astype(jnp.float32)
    inv = lax.rsqrt(jnp.mean(values * values, axis=1, keepdims=True) + norm_eps)
    normed_own = (values * inv * final_gain).astype(jnp.bfloat16)
    normed = whole_of(normed_own, VP, (1, 0, 2), 0)
    ncols = vocab.shape[1]
    scores = jnp.dot(normed, vocab, preferred_element_type=jnp.float32) + vocab_bias
    local_top = jnp.max(scores, axis=1)
    local_total = jnp.sum(jnp.exp(scores - local_top[:, None]), axis=1)
    column_ids = lax.broadcasted_iota(jnp.int32, (group, ncols), 1) + mine * ncols
    hit = column_ids == targets[:, None]
    local_target = jnp.sum(jnp.where(hit, scores, 0.0), axis=1)
    top, total, target_score = merged_by_axis(
        (local_top, local_total, local_target), VP, combine_stats
    )
    lse = top + jnp.log(total)
    group_losses = lse - target_score + zloss_weight * lse * lse
    losses = lax.dynamic_slice_in_dim(group_losses, mine * rows_dev, rows_dev)
    probs = jnp.exp(scores - lse[:, None])
    dscore = (probs * (1.0 + 2.0 * zloss_weight * lse)[:, None] - jnp.where(hit, 1.0, 0.0)).astype(
        jnp.bfloat16
    )
    feat_group = width // lax.axis_size("dp")
    feat_start = lax.axis_index("dp") * feat_group
    pieces = sent_together((normed, dscore), "dp", 0, 1)
    rows_slice = lax.dynamic_slice_in_dim(pieces[0], feat_start, feat_group, 1)
    grad_vocab = lax.dot_general(
        rows_slice, pieces[1], (((0,), (0,)), ((), ())), preferred_element_type=jnp.float32
    )
    row_term = lax.dot_general(
        dscore, vocab, (((1,), (1,)), ((), ())), preferred_element_type=jnp.float32
    )
    row_parts = lax.all_to_all(
        row_term[:, None, :].astype(jnp.bfloat16), VP, split_axis=0, concat_axis=1, tiled=True
    ).astype(jnp.float32)
    dnormed = jnp.sum(row_parts, axis=1)
    scaled = dnormed * final_gain
    grad_input = inv * (
        scaled - values * inv * inv * jnp.mean(values * scaled, axis=1, keepdims=True)
    )
    return (losses, grad_input, grad_vocab)


def solution(mesh):
    torus = Mesh(mesh.devices.reshape(16, 4, 2, mesh.shape["dp"]), ("vp_0", "vp_1", "vp_2", "dp"))
    return jax.shard_map(
        body,
        mesh=torus,
        in_specs=(P(DP_VP, None), P("dp", VP), P(None, VP), P(), P(None, VP), P(VP), P("dp")),
        out_specs=(P(DP_VP), P(DP_VP, None), P("dp", VP)),
        check_vma=False,
    )
```

profile of v0, /device:TPU:57, one launch (start us, length us, event | category | flops | bytes accessed | tf_op | source)
XLA Modules:
  0.0 377.8 jit_solution(5065636591865383652)
XLA Ops:
  7.2 2.5 all_to_all.30
  10.1 0.8 reshape.1388
  10.9 38.9 %all_to_all.40 = bf16[128,2,352]{2,1,0:T(2,128)(2,1)S(1)} all-to-all(bf16[128,2,352]{2,1,0:T(2,128)(2,1)S(1)} %reshape.1388), channel_id=1, replica_groups=mesh['vp_0'=16,'vp_1'=4,'vp_2'=2,'dp'=4] {'vp_0','vp_1','vp_2'}, dimensions={0} | all-to-all | bytes 360448 | tf_op jit(solution)/shard_map/all_to_all | solution.py:81
  49.8 0.5 reshape.1389
  50.8 2.2 copy.15
  53.0 105.4 %all_to_all.41 = f32[256,1,2048]{2,1,0:T(1,128)S(1)} all-to-all(f32[256,1,2048]{2,1,0:T(1,128)S(1)} %copy.15), channel_id=1, replica_groups=mesh['vp_0'=16,'vp_1'=4,'vp_2'=2,'dp'=4] {'vp_0','vp_1','vp_2'}, dimensions={0} | all-to-all | bytes 4194304 | tf_op jit(solution)/shard_map/all_to_all | solution.py:83
  158.4 6.8 %reduce.6 = f32[256,2048]{1,0:T(8,128)} reduce(f32[256,1,2048]{2,1,0:T(1,128)S(1)} %all_to_all.41, f32[]{:T(128)} %constant.50), dimensions={1}, to_apply=%all_to_all.34.reduce_sub_computation | reduce | bytes 4194308 | tf_op jit(solution)/shard_map/all_to_all | solution.py:83
  165.2 2.5 all_to_all.35
  167.7 0.7 reduce_sum.54
  168.7 9.1 %all-gather.4 = bf16[4,2,2048]{2,1,0:T(2,128)(2,1)S(1)} all-gather(bf16[1,2,2048]{2,1,0:T(2,128)(2,1)S(1)} %fusion.15), channel_id=2, replica_groups=mesh['vp_0'=16,'vp_1'=4,'vp_2'=2,'dp'=4] {'vp_1'}, dimensions={0}, use_global_device_ids=true | all-gather | bytes 40960 | tf_op jit(solution)/shard_map/all_gather | solution.py:24
  177.7 25.1 %all_gather.31 = bf16[64,2,2048]{2,1,0:T(2,128)(2,1)} all-gather(bf16[4,2,2048]{2,1,0:T(2,128)(2,1)S(1)} %all-gather.4), channel_id=1, replica_groups=mesh['vp_0'=16,'vp_1'=4,'vp_2'=2,'dp'=4] {'vp_0'}, dimensions={0}, use_global_device_ids=true | all-gather | bytes 557056 | tf_op jit(solution)/shard_map/all_gather | solution.py:24
  202.9 24.1 %all-gather.11.cloned.1.call-done = bf16[128,2,2048]{2,1,0:T(2,128)(2,1)} async-done(((bf16[64,2,2048]{2,1,0:T(2,128)(2,1)}), bf16[128,2,2048]{2,1,0:T(2,128)(2,1)}) %all-gather.11.cloned.1.call-update) | async-done | bytes 1048592 | tf_op jit(solution)/shard_map/all_gather | solution.py:24
  227.0 2.4 copy.23
  229.9 0.6 fusion.96
  230.7 22.2 %all-gather.5 = f32[16,3,256]{2,1,0:T(4,128)S(1)} all-gather(f32[1,3,256]{2,1,0:T(4,128)S(1)} %maximum_bitcast_fusion), channel_id=3, replica_groups=mesh['vp_0'=16,'vp_1'=4,'vp_2'=2,'dp'=4] {'vp_0'}, dimensions={0}, use_global_device_ids=true | all-gather | bytes 52224 | tf_op jit(solution)/shard_map/all_gather | solution.py:43
  252.9 9.4 %all-gather.6 = f32[4,3,256]{2,1,0:T(4,128)S(1)} all-gather(f32[1,3,256]{2,1,0:T(4,128)S(1)} %maximum_bitcast_fusion.1), channel_id=4, replica_groups=mesh['vp_0'=16,'vp_1'=4,'vp_2'=2,'dp'=4] {'vp_1'}, dimensions={0}, use_global_device_ids=true | all-gather | bytes 15360 | tf_op jit(solution)/shard_map/all_gather | solution.py:43
  262.4 11.5 %all-gather.7 = f32[2,3,256]{2,1,0:T(4,128)S(1)} all-gather(f32[1,3,256]{2,1,0:T(4,128)S(1)} %maximum_bitcast_fusion.2), channel_id=5, replica_groups=mesh['vp_0'=16,'vp_1'=4,'vp_2'=2,'dp'=4] {'vp_2'}, dimensions={0}, use_global_device_ids=true | all-gather | bytes 9216 | tf_op jit(solution)/shard_map/all_gather | solution.py:43
  274.2 1.1 pad_maximum_fusion
  275.3 0.5 fusion
  275.8 0.5 broadcast.44
  276.3 1.4 reduce.9
  277.7 1.5 reshape.1390
  279.3 14.1 %all-to-all-start.2 = ((bf16[128,2,2048]{2,1,0:T(2,128)(2,1)}), bf16[128,2,2048]{2,1,0:T(2,128)(2,1)}, u32[]{:S(2)}, u32[]{:S(2)}) async-start(bf16[128,2,2048]{2,1,0:T(2,128)(2,1)} %reshape.1390), calls=%async_computation.2 | async-start | bytes 2097152 | tf_op jit(solution)/shard_map/all_to_all | solution.py:117
  293.3 0.6 dynamic_slice.6
  293.9 54.6 %all-to-all-done.2 = bf16[128,2,2048]{2,1,0:T(2,128)(2,1)} async-done(((bf16[128,2,2048]{2,1,0:T(2,128)(2,1)}), bf16[128,2,2048]{2,1,0:T(2,128)(2,1)}, u32[]{:S(2)}, u32[]{:S(2)}) %all-to-all-start.2) | async-done | bytes 1048608 | tf_op jit(solution)/shard_map/all_to_all | solution.py:117
  348.5 6.5 %reshape.1391 = bf16[256,1,2048]{2,1,0:T(2,128)(2,1)S(1)} reshape(bf16[128,2,2048]{2,1,0:T(2,128)(2,1)} %all-to-all-done.2) | data formatting | bytes 2097152
  355.0 7.4 %convert_reduce_fusion = f32[256,2048]{1,0:T(8,128)} fusion(bf16[256,1,2048]{2,1,0:T(2,128)(2,1)S(1)} %reshape.1391), kind=kLoop, calls=%fused_computation.3 | loop fusion | flops 524288 | bytes 3145728 | tf_op jit(solution)/shard_map/convert_element_type | solution.py:119
  362.4 2.5 reshape.1359
  364.9 0.7 reduce_sum.58
  365.8 0.7 fusion.12
  366.5 2.2 slice-done
  368.6 2.3 fusion.1
  (40 shorter events, 2.3 us)
Async XLA Ops:
  7.2 222.8 %copy-start = (bf16[2048,256]{1,0:T(8,128)(2,1)S(1)}, bf16[2048,256]{1,0:T(8,128)(2,1)}, u32[]{:S(2)}) copy-start(bf16[2048,256]{1,0:T(8,128)(2,1)} %param.11) | copy-start | bytes 3145732
  7.2 43.1 %copy-start.2 = (bf16[256,44]{0,1:T(8,128)(2,1)S(1)}, bf16[256,44]{0,1:T(8,128)(2,1)}, u32[]{:S(2)}) copy-start(bf16[256,44]{0,1:T(8,128)(2,1)} %param.8) | copy-start | bytes 67588
  7.2 219.8 %all-gather.11.cloned.1.call-start = ((), (), s32[]{:S(2)}) async-start(), calls=%async_computation.3 | async-start | bytes 1572864 | tf_op jit(solution)/shard_map/all_gather | solution.py:24
  167.7 0.8 copy-start.3
  167.7 0.9 copy-start.1
  202.9 163.6 %all-gather.13.cloned.1.call-start = ((), (), s32[]{:S(2)}) async-start(), calls=%async_computation.4 | async-start | bytes 5898240 | tf_op jit(solution)/shard_map/all_gather | solution.py:67
  227.0 2.9 copy-start.5
  229.5 1.1 copy-start.4
  279.3 69.3 %all-to-all-start.2 = ((bf16[128,2,2048]{2,1,0:T(2,128)(2,1)}), bf16[128,2,2048]{2,1,0:T(2,128)(2,1)}, u32[]{:S(2)}, u32[]{:S(2)}) async-start(bf16[128,2,2048]{2,1,0:T(2,128)(2,1)} %reshape.1390), calls=%async_computation.2 | async-start | bytes 2097152 | tf_op jit(solution)/shard_map/all_to_all | solution.py:117
  366.4 2.2 slice-start
Sparse Core Ops, SparseCore 0:
  203.0 23.9 all-gather.10
  275.4 56.7 all-gather.12
where the time goes:
time: 379 us; the launch traced here: 378 us
  blocking collectives  222 us (59%)
  waiting for transfers between devices  78.7 us (21%)
  local copies, waits for them, and re-layouts  25.6 us (7%)
  other arithmetic  19.6 us (5%)
  between operations  14.3 us (4%)
  starting transfers between devices  14.1 us (4%)
  matrix products  3.84 us (1%)
    all_to_all x1, blocking collectives, body(): lax.all_to_all(partial_value[:, None, :], VP, split_axis=0, concat_axis=1...  105 us
    all_to_all x1, waiting for transfers between devices, body(): lax.all_to_all(row_term[:, None, :].astype(jnp.bfloat16), VP, split_axis=...  54.6 us
    all_gather x3, blocking collectives, collected_together(): both, at, found = (lax.all_gather(jnp.concatenate(lines), axis), 0, {})  43.1 us
    all_to_all x1, blocking collectives, body(): w_rows = lax.all_to_all(w_down, VP, split_axis=0, concat_axis=1, tiled=True)  38.9 us
    all_gather x2, blocking collectives, gather_in_order(): pieces = lax.all_gather(pieces, axes[k], axis=0, tiled=True)  34.2 us
    all_gather x1, waiting for transfers between devices, gather_in_order(): pieces = lax.all_gather(pieces, axes[k], axis=0, tiled=True)  24.1 us
    all_to_all x1, starting transfers between devices, body(): lax.all_to_all(row_term[:, None, :].astype(jnp.bfloat16), VP, split_axis=...  14.1 us
    unnamed x16, local copies, waits for them, and re-layouts  9.37 us
  transfers between devices with their start and end apart: 3, of which 2 were waited for; matrix products, arithmetic and copies ran while one was open for 6% of the time, Pallas kernels for 0%

commit v1 on v0

v1 whole, which is shorter than its diff:
```python
import jax
import jax.numpy as jnp
from jax import lax
from jax.sharding import Mesh
from jax.sharding import PartitionSpec as P

Z = "vp_0"
Q = ("vp_1", "vp_2")
VP = ("vp_0", "vp_1", "vp_2")
DP_VP = ("dp", "vp_0", "vp_1", "vp_2")

norm_eps = 1e-06
zloss_weight = 0.001
f32 = jnp.float32
bf16 = jnp.bfloat16


def exchange(blocks, axes):
    return lax.all_to_all(blocks, axes, split_axis=0, concat_axis=0, tiled=True)


def shared(block, axes, count):
    return exchange(jnp.broadcast_to(block[None], (count, *block.shape)), axes)


def dot(a, b, da, db):
    return lax.dot_general(a, b, (((da,), (db,)), ((), ())), preferred_element_type=f32)


def merged(stats):
    top = jnp.max(stats[:, 0], axis=0)
    lse = top + jnp.log(jnp.sum(jnp.exp(stats[:, 0] - top), axis=0))
    return jnp.stack([lse, jnp.sum(stats[:, 1], axis=0)])


def body(stream, hidden, w_down, final_gain, vocab, vocab_bias, targets):
    nz, nq = lax.axis_size(Z), lax.axis_size(Q)
    ny = lax.axis_size("dp")
    own, width = stream.shape
    group, units = hidden.shape
    cols = w_down.shape[1]
    ncols = vocab.shape[1]
    z, mine = lax.axis_index(Z), lax.axis_index(VP)
    feats = nz * cols
    span = nq * own
    part = stream.reshape(own, nz, nq, cols).transpose(2, 0, 1, 3).reshape(nq, own, feats)
    units_all = jnp.broadcast_to(hidden.T[None], (nq, units, group))
    first = exchange(jnp.concatenate([units_all, part], axis=1), Q)
    hid = first[:, :units].reshape(nq * units, group)
    rows = first[:, units:].reshape(span, feats)
    w_rows = exchange(w_down.T.reshape(cols, nz, nq * units).transpose(1, 0, 2), Z)
    w_rows = w_rows.reshape(feats, nq * units)
    place = lax.broadcasted_iota(jnp.int32, (span, group), 1) - z * span
    place = (place == lax.broadcasted_iota(jnp.int32, (span, group), 0)).astype(bf16)
    partial = dot(w_rows, hid, 1, 0) + dot(rows, place, 0, 0)
    arrived = exchange(partial.reshape(nz, cols, group), Z)
    normin = jnp.sum(arrived, axis=0).astype(bf16)
    by_z = shared(normin, Z, nz)
    by_q = shared(by_z, Q, nq)
    normin = by_q.transpose(1, 0, 2, 3).reshape(width, group)
    values = normin.astype(f32)
    inv = lax.rsqrt(jnp.mean(values * values, axis=0, keepdims=True) + norm_eps)
    normed = (values * inv * final_gain[:, None]).astype(bf16)

    scores = dot(vocab, normed, 0, 0) + vocab_bias[:, None]
    top = jnp.max(scores, axis=0)
    local = top + jnp.log(jnp.sum(jnp.exp(scores - top), axis=0))
    ids = lax.broadcasted_iota(jnp.int32, (ncols, group), 0) + mine * ncols
    hit = ids == targets[None, :]
    goal = jnp.sum(jnp.where(hit, scores, 0.0), axis=0)
    stats = merged(shared(jnp.stack([local, goal]), Q, nq))
    stats = merged(shared(stats, Z, nz))
    lse = stats[0]
    losses = lse - stats[1] + zloss_weight * lse * lse
    losses = lax.dynamic_slice_in_dim(losses, mine * own, own)
    dscore = (jnp.exp(scores - lse) * (1.0 + 2.0 * zloss_weight * lse) - jnp.where(hit, 1.0, 0.0)).astype(bf16)

    feat_group = width // ny
    normed_y = exchange(normed.reshape(ny, feat_group, group), "dp")
    dscore_y = shared(dscore, "dp", ny)
    grad_vocab = sum(dot(normed_y[g], dscore_y[g], 1, 1) for g in range(ny))

    line = lax.broadcasted_iota(jnp.int32, (group, group), 0)
    token = (line // own) % nz * span + line // (own * nz) * own + line % own
    order = (token == lax.broadcasted_iota(jnp.int32, (group, group), 1)).astype(bf16)
    dscore_rows = dot(order, dscore, 1, 1).astype(bf16)
    row_term = dot(dscore_rows, vocab, 1, 1).astype(bf16)
    row_q = exchange(row_term.reshape(nq, nz * own, width), Q)
    row_q = jnp.sum(row_q.astype(f32), axis=0).astype(bf16)
    row_z = exchange(row_q.reshape(nz, own, width), Z)
    dnormed = jnp.sum(row_z.astype(f32), axis=0)

    pick = lax.broadcasted_iota(jnp.int32, (own, group), 0) + mine * own
    pick = (pick == lax.broadcasted_iota(jnp.int32, (own, group), 1)).astype(bf16)
    values = dot(pick, normin, 1, 1)
    inv = lax.rsqrt(jnp.mean(values * values, axis=1, keepdims=True) + norm_eps)
    scaled = dnormed * final_gain
    grad_input = inv * (
        scaled - values * inv * inv * jnp.mean(values * scaled, axis=1, keepdims=True)
    )
    return (losses, grad_input, grad_vocab)


def solution(mesh):
    torus = Mesh(mesh.devices.reshape(16, 4, 2, mesh.shape["dp"]), ("vp_0", "vp_1", "vp_2", "dp"))
    return jax.shard_map(
        body,
        mesh=torus,
        in_specs=(P(DP_VP, None), P("dp", VP), P(None, VP), P(), P(None, VP), P(VP), P("dp")),
        out_specs=(P(DP_VP), P(DP_VP, None), P("dp", VP)),
        check_vma=False,
    )
```

time: 379 us -> 207 us (0.55)
  the two profiles are of different devices: /device:TPU:57 before, /device:TPU:32 now
where the time goes in v1:
time: 207 us; the launch traced here: 206 us
  waiting for transfers between devices  75.7 us (37%)
  blocking collectives  67.2 us (32%)
  starting transfers between devices  39.2 us (19%)
  matrix products  10.1 us (5%)
  local copies, waits for them, and re-layouts  7.1 us (3%)
  other arithmetic  5.47 us (3%)
    all_to_all x7, waiting for transfers between devices, exchange(): return lax.all_to_all(blocks, axes, split_axis=0, concat_axis=0, tiled=True)  75.7 us
    all_to_all x4, blocking collectives, exchange(): return lax.all_to_all(blocks, axes, split_axis=0, concat_axis=0, tiled=True)  67.2 us
    all_to_all x7, starting transfers between devices, exchange(): return lax.all_to_all(blocks, axes, split_axis=0, concat_axis=0, tiled=True)  39.2 us
    dot_general x9, matrix products, dot(): lax.dot_general(a, b, (((da,), (db,)), ((), ())), preferred_element_type=...  10.1 us
  transfers between devices with their start and end apart: 7, of which 7 were waited for; matrix products, arithmetic and copies ran while one was open for 6% of the time, Pallas kernels for 0%

profile of v1, /device:TPU:32, one launch (start us, length us, event | category | flops | bytes accessed | tf_op | source)
XLA Modules:
  0.0 205.7 jit_solution(7416464949970944997)
XLA Ops:
  0.6 0.9 reshape.128
  1.7 0.8 broadcast_in_dim.20
  3.2 4.3 %all-to-all-start = ((bf16[8,46,256]{2,1,0:T(8,128)(2,1)}), bf16[8,46,256]{2,1,0:T(8,128)(2,1)S(1)}, u32[]{:S(2)}, u32[]{:S(2)}) async-start(bf16[8,46,256]{2,1,0:T(8,128)(2,1)} %pad_maximum_fusion), calls=%async_computation | async-start | bytes 393216 | tf_op jit(solution)/shard_map/all_to_all | solution.py:19
  7.5 1.2 reshape.131
  9.4 4.9 %all-to-all-done = bf16[8,46,256]{2,1,0:T(8,128)(2,1)S(1)} async-done(((bf16[8,46,256]{2,1,0:T(8,128)(2,1)}), bf16[8,46,256]{2,1,0:T(8,128)(2,1)S(1)}, u32[]{:S(2)}, u32[]{:S(2)}) %all-to-all-start) | async-done | bytes 188448 | tf_op jit(solution)/shard_map/all_to_all | solution.py:19
  14.3 15.2 %all-to-all-start.1 = ((bf16[16,16,352]{2,1,0:T(8,128)(2,1)}), bf16[16,16,352]{2,1,0:T(8,128)(2,1)S(1)}, u32[]{:S(2)}, u32[]{:S(2)}) async-start(bf16[16,16,352]{2,1,0:T(8,128)(2,1)} %bitcast.85), calls=%async_computation.1 | async-start | bytes 393216 | tf_op jit(solution)/shard_map/all_to_all | solution.py:19
  29.8 14.9 %all-to-all-done.1 = bf16[16,16,352]{2,1,0:T(8,128)(2,1)S(1)} async-done(((bf16[16,16,352]{2,1,0:T(8,128)(2,1)}), bf16[16,16,352]{2,1,0:T(8,128)(2,1)S(1)}, u32[]{:S(2)}, u32[]{:S(2)}) %all-to-all-start.1) | async-done | bytes 180256 | tf_op jit(solution)/shard_map/all_to_all | solution.py:19
  44.9 23.7 %all_to_all.55 = f32[16,16,256]{2,1,0:T(8,128)S(1)} all-to-all(f32[16,16,256]{2,1,0:T(8,128)S(1)} %bitcast.91), channel_id=1, replica_groups=mesh['vp_0'=16,'vp_1'=4,'vp_2'=2,'dp'=4] {'vp_0'}, dimensions={0} | all-to-all | bytes 524288 | tf_op jit(solution)/shard_map/all_to_all | solution.py:19
  68.6 20.0 %all_to_all.56 = bf16[16,16,256]{2,1,0:T(8,128)(2,1)S(1)} all-to-all(bf16[16,16,256]{2,1,0:T(8,128)(2,1)S(1)} %broadcast_in_dim.21), channel_id=1, replica_groups=mesh['vp_0'=16,'vp_1'=4,'vp_2'=2,'dp'=4] {'vp_0'}, dimensions={0} | all-to-all | bytes 262144 | tf_op jit(solution)/shard_map/all_to_all | solution.py:19
  88.6 1.1 broadcast_in_dim.22
  89.7 3.6 %all-to-all-start.4 = ((bf16[8,16,16,256]{3,2,1,0:T(8,128)(2,1)}), bf16[8,16,16,256]{3,2,1,0:T(8,128)(2,1)S(1)}, u32[]{:S(2)}, u32[]{:S(2)}) async-start(bf16[8,16,16,256]{3,2,1,0:T(8,128)(2,1)} %broadcast_in_dim.22), calls=%async_computation.4 | async-start | bytes 2097152 | tf_op jit(solution)/shard_map/all_to_all | solution.py:19
  93.3 15.8 %all-to-all-done.4 = bf16[8,16,16,256]{3,2,1,0:T(8,128)(2,1)S(1)} async-done(((bf16[8,16,16,256]{3,2,1,0:T(8,128)(2,1)}), bf16[8,16,16,256]{3,2,1,0:T(8,128)(2,1)S(1)}, u32[]{:S(2)}, u32[]{:S(2)}) %all-to-all-start.4) | async-done | bytes 1048608 | tf_op jit(solution)/shard_map/all_to_all | solution.py:19
  109.4 1.7 bitcast_convert_fusion
  111.1 0.9 fusion.73
  112.2 7.8 %all_to_all.57 = f32[8,2,256]{2,1,0:T(2,128)S(1)} all-to-all(f32[8,2,256]{2,1,0:T(2,128)S(1)} %broadcast_in_dim.24), channel_id=1, replica_groups=mesh['vp_0'=16,'vp_1'=4,'vp_2'=2,'dp'=4] {'vp_1','vp_2'}, dimensions={0} | all-to-all | bytes 32768 | tf_op jit(solution)/shard_map/all_to_all | solution.py:19
  120.1 15.7 %all_to_all.58 = f32[16,2,256]{2,1,0:T(2,128)S(1)} all-to-all(f32[16,2,256]{2,1,0:T(2,128)S(1)} %broadcast_in_dim.25), channel_id=1, replica_groups=mesh['vp_0'=16,'vp_1'=4,'vp_2'=2,'dp'=4] {'vp_0'}, dimensions={0} | all-to-all | bytes 65536 | tf_op jit(solution)/shard_map/all_to_all | solution.py:19
  136.0 0.8 broadcast_in_dim.27
  136.9 4.5 %all-to-all-start.10 = ((bf16[4,256,256]{2,1,0:T(8,128)(2,1)}), bf16[4,256,256]{2,1,0:T(8,128)(2,1)}, u32[]{:S(2)}, u32[]{:S(2)}) async-start(bf16[4,256,256]{2,1,0:T(8,128)(2,1)} %broadcast_in_dim.27), calls=%async_computation.10 | async-start | bytes 1048576 | tf_op jit(solution)/shard_map/all_to_all | solution.py:19
  141.3 1.4 multiply_convert_fusion
  142.7 6.8 %all-to-all-done.10 = bf16[4,256,256]{2,1,0:T(8,128)(2,1)} async-done(((bf16[4,256,256]{2,1,0:T(8,128)(2,1)}), bf16[4,256,256]{2,1,0:T(8,128)(2,1)}, u32[]{:S(2)}, u32[]{:S(2)}) %all-to-all-start.10) | async-done | bytes 524320 | tf_op jit(solution)/shard_map/all_to_all | solution.py:19
  149.5 3.5 %all-to-all-start.9 = ((bf16[4,512,256]{2,1,0:T(8,128)(2,1)}), bf16[4,512,256]{2,1,0:T(8,128)(2,1)S(1)}, u32[]{:S(2)}, u32[]{:S(2)}) async-start(bf16[4,512,256]{2,1,0:T(8,128)(2,1)} %multiply_convert_fusion), calls=%async_computation.9 | async-start | bytes 2097152 | tf_op jit(solution)/shard_map/all_to_all | solution.py:19
  153.1 1.9 convolution_convert_fusion
  155.0 10.6 %all-to-all-done.9 = bf16[4,512,256]{2,1,0:T(8,128)(2,1)S(1)} async-done(((bf16[4,512,256]{2,1,0:T(8,128)(2,1)}), bf16[4,512,256]{2,1,0:T(8,128)(2,1)S(1)}, u32[]{:S(2)}, u32[]{:S(2)}) %all-to-all-start.9) | async-done | bytes 1048608 | tf_op jit(solution)/shard_map/all_to_all | solution.py:19
  165.5 3.6 %all-to-all-start.7 = ((bf16[8,32,2048]{2,1,0:T(8,128)(2,1)}), bf16[8,32,2048]{2,1,0:T(8,128)(2,1)S(1)}, u32[]{:S(2)}, u32[]{:S(2)}) async-start(bf16[8,32,2048]{2,1,0:T(8,128)(2,1)} %bitcast.92), calls=%async_computation.7 | async-start | bytes 2097152 | tf_op jit(solution)/shard_map/all_to_all | solution.py:19
  169.7 1.2 fusion.11
  170.9 2.0 convolution_add_fusion.2
  172.8 12.1 %all-to-all-done.7 = bf16[8,32,2048]{2,1,0:T(8,128)(2,1)S(1)} async-done(((bf16[8,32,2048]{2,1,0:T(8,128)(2,1)}), bf16[8,32,2048]{2,1,0:T(8,128)(2,1)S(1)}, u32[]{:S(2)}, u32[]{:S(2)}) %all-to-all-start.7) | async-done | bytes 1048608 | tf_op jit(solution)/shard_map/all_to_all | solution.py:19
  185.1 0.7 reshape.137
  185.9 4.6 %all-to-all-start.8 = ((bf16[16,2,2048]{2,1,0:T(2,128)(2,1)}), bf16[16,2,2048]{2,1,0:T(2,128)(2,1)S(1)}, u32[]{:S(2)}, u32[]{:S(2)}) async-start(bf16[16,2,2048]{2,1,0:T(2,128)(2,1)} %reshape.137), calls=%async_computation.8 | async-start | bytes 262144 | tf_op jit(solution)/shard_map/all_to_all | solution.py:19
  190.4 1.4 convolution_add_fusion.1
  191.8 2.0 convolution_add_fusion
  193.8 10.7 %all-to-all-done.8 = bf16[16,2,2048]{2,1,0:T(2,128)(2,1)S(1)} async-done(((bf16[16,2,2048]{2,1,0:T(2,128)(2,1)}), bf16[16,2,2048]{2,1,0:T(2,128)(2,1)S(1)}, u32[]{:S(2)}, u32[]{:S(2)}) %all-to-all-start.8) | async-done | bytes 131104 | tf_op jit(solution)/shard_map/all_to_all | solution.py:19
  (58 shorter events, 4.9 us)
Async XLA Ops:
  0.6 110.5 %copy-start = (bf16[2048,256]{1,0:T(8,128)(2,1)S(1)}, bf16[2048,256]{1,0:T(8,128)(2,1)}, u32[]{:S(2)}) copy-start(bf16[2048,256]{1,0:T(8,128)(2,1)} %param.11) | copy-start | bytes 3145732
  3.2 11.1 %all-to-all-start = ((bf16[8,46,256]{2,1,0:T(8,128)(2,1)}), bf16[8,46,256]{2,1,0:T(8,128)(2,1)S(1)}, u32[]{:S(2)}, u32[]{:S(2)}) async-start(bf16[8,46,256]{2,1,0:T(8,128)(2,1)} %pad_maximum_fusion), calls=%async_computation | async-start | bytes 393216 | tf_op jit(solution)/shard_map/all_to_all | solution.py:19
  14.3 30.4 %all-to-all-start.1 = ((bf16[16,16,352]{2,1,0:T(8,128)(2,1)}), bf16[16,16,352]{2,1,0:T(8,128)(2,1)S(1)}, u32[]{:S(2)}, u32[]{:S(2)}) async-start(bf16[16,16,352]{2,1,0:T(8,128)(2,1)} %bitcast.85), calls=%async_computation.1 | async-start | bytes 393216 | tf_op jit(solution)/shard_map/all_to_all | solution.py:19
  89.7 19.4 %all-to-all-start.4 = ((bf16[8,16,16,256]{3,2,1,0:T(8,128)(2,1)}), bf16[8,16,16,256]{3,2,1,0:T(8,128)(2,1)S(1)}, u32[]{:S(2)}, u32[]{:S(2)}) async-start(bf16[8,16,16,256]{3,2,1,0:T(8,128)(2,1)} %broadcast_in_dim.22), calls=%async_computation.4 | async-start | bytes 2097152 | tf_op jit(solution)/shard_map/all_to_all | solution.py:19
  109.4 1.7 copy-start.4
  109.4 1.7 copy-start.6
  111.1 24.9 %copy-start.2 = (bf16[8,16,16,256]{3,2,0,1:T(8,128)(2,1)}, bf16[8,16,16,256]{3,2,0,1:T(8,128)(2,1)S(1)}, u32[]{:S(2)}) copy-start(bf16[8,16,16,256]{3,2,0,1:T(8,128)(2,1)S(1)} %get-tuple-element.14) | copy-start | bytes 3145732
  111.1 0.9 copy-start.5
  112.0 29.3 %copy-start.1 = (f32[16,8,16,256]{3,2,1,0:T(8,128)S(1)}, f32[16,8,16,256]{3,2,1,0:T(8,128)}, u32[]{:S(2)}) copy-start(f32[16,8,16,256]{3,2,1,0:T(8,128)} %get-tuple-element.13) | copy-start | bytes 6291460
  136.9 12.7 %all-to-all-start.10 = ((bf16[4,256,256]{2,1,0:T(8,128)(2,1)}), bf16[4,256,256]{2,1,0:T(8,128)(2,1)}, u32[]{:S(2)}, u32[]{:S(2)}) async-start(bf16[4,256,256]{2,1,0:T(8,128)(2,1)} %broadcast_in_dim.27), calls=%async_computation.10 | async-start | bytes 1048576 | tf_op jit(solution)/shard_map/all_to_all | solution.py:19
  149.5 16.0 %all-to-all-start.9 = ((bf16[4,512,256]{2,1,0:T(8,128)(2,1)}), bf16[4,512,256]{2,1,0:T(8,128)(2,1)S(1)}, u32[]{:S(2)}, u32[]{:S(2)}) async-start(bf16[4,512,256]{2,1,0:T(8,128)(2,1)} %multiply_convert_fusion), calls=%async_computation.9 | async-start | bytes 2097152 | tf_op jit(solution)/shard_map/all_to_all | solution.py:19
  165.5 19.4 %all-to-all-start.7 = ((bf16[8,32,2048]{2,1,0:T(8,128)(2,1)}), bf16[8,32,2048]{2,1,0:T(8,128)(2,1)S(1)}, u32[]{:S(2)}, u32[]{:S(2)}) async-start(bf16[8,32,2048]{2,1,0:T(8,128)(2,1)} %bitcast.92), calls=%async_computation.7 | async-start | bytes 2097152 | tf_op jit(solution)/shard_map/all_to_all | solution.py:19
  185.1 19.4 %copy-start.3 = (bf16[8,16,16,256]{3,2,0,1:T(8,128)(2,1)S(1)}, bf16[8,16,16,256]{3,2,0,1:T(8,128)(2,1)}, u32[]{:S(2)}) copy-start(bf16[8,16,16,256]{3,2,0,1:T(8,128)(2,1)} %copy-done.2) | copy-start | bytes 3145732
  185.9 18.6 %all-to-all-start.8 = ((bf16[16,2,2048]{2,1,0:T(2,128)(2,1)}), bf16[16,2,2048]{2,1,0:T(2,128)(2,1)S(1)}, u32[]{:S(2)}, u32[]{:S(2)}) async-start(bf16[16,2,2048]{2,1,0:T(2,128)(2,1)} %reshape.137), calls=%async_computation.8 | async-start | bytes 262144 | tf_op jit(solution)/shard_map/all_to_all | solution.py:19
